TPU v7x, 32 devices: a whole 2x2x4 slice. The times are simulated.
32 devices in a mesh: fs: 8 (over z, x), tp: 4 (over y, core).
Axes of the slice: x: 2, y: 2, z: 4, core: 2. Of those that a mesh axis runs over, the one named last changes fastest.
Arguments:
- tokens: bfloat16 [8192, 2048], P(('fs', 'tp')), may hold values from -130 to 130
- pool_weight: bfloat16 [4, 512, 512], P(None, 'fs'), may hold values from -0.25 to 0.25
- pool_scale: float32 [2048], replicated, may hold values from 0.5 to 1.5
- gain_mix: float32 [2048], replicated, may hold values from 0.1 to 1.9
- gain_mlp: float32 [2048], replicated, may hold values from 0.1 to 1.9
- w_up: bfloat16 [8192, 2048], P('tp', 'fs'), may hold values from -0.125 to 0.125
- w_down: bfloat16 [8192, 2048], P('tp', 'fs'), may hold values from -0.0625 to 0.0625
- gain_out: float32 [2048], P('tp'), may hold values from 0.1 to 1.9
Outputs:
- result: bfloat16 [8192, 2048], P('fs', 'tp')
All inputs are finite; a program needn't handle non-finite values.
Results may differ from a plain program's by a relative error of at most 0.013.
Values may be sent and summed in bfloat16 or wider, within the bound.
A program may use at most 64 MiB of HBM per device.

v0:
```python
import jax
import jax.numpy as jnp
from jax import lax
from jax.sharding import PartitionSpec as P

D = 2048
SEQ_LEN = 1024
EPS = 1e-06
WINDOWS = (2, 4, 8, 16)


def extended_2(x, sides, width):
    for axis, dim in sides:
        peers, length = (lax.axis_size(axis), x.shape[dim])
        up = [(i, (i + 1) % peers) for i in range(peers - 1)]
        down = [(j, i) for i, j in up]
        last = lax.slice_in_dim(x, length - width, length, axis=dim)
        first = lax.slice_in_dim(x, 0, width, axis=dim)
        before = lax.ppermute(last, axis, up)
        after = lax.ppermute(first, axis, down)
        x = jnp.concatenate([before, x, after], axis=dim)
    return x


def rms_scale(values, gain):
    return values * lax.rsqrt(jnp.mean(values * values, axis=-1, keepdims=True) + EPS) * gain


def local(tokens, pool_weight, pool_scale, gain_mix, gain_mlp, w_up, w_down, gain_out):
    rows = tokens.shape[0]
    width = tokens.shape[1]
    group = width // 4
    offset = lax.axis_index("tp") * rows
    inputs = tokens.astype(jnp.float32)
    normed = rms_scale(inputs, gain_mix).astype(jnp.bfloat16)
    extended = extended_2(normed, (("tp", 0),), 8).astype(jnp.float32)
    line = jnp.arange(rows + 16, dtype=jnp.int32)
    lower_open = offset % SEQ_LEN != 0
    upper_open = (offset + rows) % SEQ_LEN != 0
    keep = jnp.where(line < 8, lower_open, jnp.where(line >= rows + 8, upper_open, True))
    level = extended * keep.astype(jnp.float32)[:, None]
    position = (offset + jnp.arange(rows, dtype=jnp.int32)) % SEQ_LEN
    normed_f32 = normed.astype(jnp.float32)
    full_pool = lax.all_gather(pool_weight, "fs", axis=1, tiled=True)
    pieces = []
    for index, reach in enumerate(WINDOWS):
        half = reach // 2
        level = level[:-half] + level[half:]
        start = 8 - half
        window = level[start : start + rows, :group]
        lower = jnp.maximum(position - half, 0)
        upper = jnp.minimum(position + half, SEQ_LEN)
        counts = (upper - lower).astype(jnp.float32)[:, None]
        own = normed_f32[:, index * group : (index + 1) * group]
        pooled = (window / counts - own).astype(jnp.bfloat16)
        pieces.append(jnp.dot(pooled, full_pool[index], preferred_element_type=jnp.float32))
        level = level[:, group:]
    mixed = jnp.concatenate(pieces, axis=1) * pool_scale
    first_sum = (inputs + mixed).astype(jnp.bfloat16)
    inner = rms_scale(first_sum.astype(jnp.float32), gain_mlp).astype(jnp.bfloat16)
    all_inner = lax.all_gather(inner, "tp", axis=0, tiled=True)
    contract = (((1,), (1,)), ((), ()))
    pre = lax.dot_general(
        all_inner,
        lax.all_gather(w_up, "fs", axis=1, tiled=True),
        contract,
        preferred_element_type=jnp.float32,
    )
    hidden = jnp.square(jax.nn.relu(pre)).astype(jnp.bfloat16)
    partial_terms = jnp.dot(
        hidden, lax.all_gather(w_down, "fs", axis=1, tiled=True), preferred_element_type=jnp.float32
    )
    channel_out = lax.psum_scatter(
        partial_terms.astype(jnp.bfloat16), "tp", scatter_dimension=1, tiled=True
    ).astype(jnp.float32)
    first_columns = lax.all_to_all(first_sum, "tp", split_axis=1, concat_axis=0, tiled=True)
    second_sum = first_columns.astype(jnp.float32) + channel_out
    squares = lax.psum(jnp.sum(second_sum * second_sum, axis=1), "tp")
    scaled = second_sum * lax.rsqrt(squares / D + EPS)[:, None] * gain_out
    return scaled.astype(jnp.bfloat16)


def solution(mesh):
    return jax.shard_map(
        local,
        mesh=mesh,
        in_specs=(
            P(("fs", "tp"), None),
            P(None, "fs", None),
            P(),
            P(),
            P(),
            P("tp", "fs"),
            P("tp", "fs"),
            P("tp"),
        ),
        out_specs=P("fs", "tp"),
        check_vma=False,
    )
```

profile of v0, /device:TPU:0, one launch (start us, length us, event | category | flops | bytes accessed | tf_op | source)
XLA Modules:
  0.0 437.5 jit_solution(9384960922146906074)
XLA Ops:
  6.5 0.7 all-gather.5.cloned.1.call-update
  7.3 1.5 fusion.3
  8.8 2.9 fusion.30
  11.7 2.4 collective-permute-start
  14.1 1.3 collective-permute-start.1
  15.5 3.8 collective-permute-done.1
  19.3 0.2 convert_multiply_fusion.4
  19.5 0.3 slice_add_fusion
  19.8 0.2 slice_add_fusion.1
  20.1 1.2 copy-done.1
  21.4 1.1 fusion.32
  22.6 38.8 %all-gather.5.cloned.1.call-done = bf16[4,512,512]{2,1,0:T(8,128)(2,1)} async-done(((bf16[4,64,512]{2,1,0:T(8,128)(2,1)}), bf16[4,512,512]{2,1,0:T(8,128)(2,1)}) %all-gather.5.cloned.1.call-update) | async-done | bytes 2097168 | tf_op jit(solution)/shard_map/all_gather | solution.py:44
  61.3 1.7 fusion.14
  63.1 0.2 copy-done.3
  63.2 1.7 fusion.12
  65.0 0.4 fusion.10
  65.4 0.6 copy-done.4
  66.2 0.4 fusion.7
  66.7 0.5 fusion
  67.2 0.2 copy-done.7
  67.4 1.3 fusion.2
  68.7 0.7 all-gather.9.cloned.1.call-update
  69.5 0.5 all-gather.11.cloned.1.call-update
  70.0 31.8 %all-gather.7.cloned.1.call-done = bf16[1024,2048]{1,0:T(8,128)(2,1)} async-done(((bf16[256,2048]{1,0:T(8,128)(2,1)}), bf16[1024,2048]{1,0:T(8,128)(2,1)}) %all-gather.7.cloned.1.call-update) | async-done | bytes 4194320 | tf_op jit(solution)/shard_map/all_gather | solution.py:61
  101.8 127.0 %all-gather.9.cloned.1.call-done = bf16[2048,2048]{1,0:T(8,128)(2,1)} async-done(((bf16[2048,256]{1,0:T(8,128)(2,1)}), bf16[2048,2048]{1,0:T(8,128)(2,1)}) %all-gather.9.cloned.1.call-update) | async-done | bytes 8388624 | tf_op jit(solution)/shard_map/all_gather | solution.py:65
  228.8 125.0 %all-gather.11.cloned.1.call-done = bf16[2048,2048]{1,0:T(8,128)(2,1)} async-done(((bf16[2048,256]{1,0:T(8,128)(2,1)}), bf16[2048,2048]{1,0:T(8,128)(2,1)}) %all-gather.11.cloned.1.call-update) | async-done | bytes 8388624 | tf_op jit(solution)/shard_map/all_gather | solution.py:71
  353.9 25.5 %convolution_convert_fusion = bf16[1024,2048]{1,0:T(8,128)(2,1)} fusion(bf16[2048,2048]{1,0:T(8,128)(2,1)} %all-gather.11.cloned.1.call-done, bf16[1024,2048]{1,0:T(8,128)(2,1)} %all-gather.7.cloned.1.call-done, bf16[2048,2048]{1,0:T(8,128)(2,1)} %all-gather.9.cloned.1.call-done), kind=kOutput, calls=%fused_computation.1 | convolution fusion | flops 17188257792 | bytes 25165824 | tf_op jit(solution)/shard_map/dot_general | solution.py:70
  379.5 17.0 %all_to_all.13 = bf16[256,4,512]{2,0,1:T(8,128)(2,1)S(1)} all-to-all(bf16[256,4,512]{2,0,1:T(8,128)(2,1)S(1)} %bitcast.28), channel_id=1, replica_groups=mesh['fs'=8,'tp'=4] {'tp'}, dimensions={1} | all-to-all | bytes 2097152 | tf_op jit(solution)/shard_map/all_to_all | solution.py:76
  396.5 25.6 %reduce-scatter.2.cloned.1.call-done = bf16[1024,512]{1,0:T(8,128)(2,1)} async-done(((bf16[1024,2048]{1,0:T(8,128)(2,1)}), bf16[1024,512]{1,0:T(8,128)(2,1)}) %reduce-scatter.2.cloned.1.call-update) | async-done | bytes 1048592 | tf_op jit(solution)/shard_map/reduce_scatter | solution.py:73
  422.1 1.7 multiply_reduce_fusion
  423.8 5.8 %psum.7 = f32[1024]{0:T(1024)S(1)} all-reduce(f32[1024]{0:T(1024)S(1)} %multiply_reduce_fusion), channel_id=1, replica_groups=mesh['fs'=8,'tp'=4] {'tp'}, use_global_device_ids=true, to_apply=%region_4.5 | all-reduce | flops 1024 | bytes 8192 | tf_op jit(solution)/shard_map/psum | solution.py:78
  429.6 1.4 multiply_convert_fusion.1
  (33 shorter events, 0.9 us)
Async XLA Ops:
  6.5 54.8 %all-gather.5.cloned.1.call-start = ((), (), s32[]{:S(2)}) async-start(), calls=%async_computation.2 | async-start | bytes 2359296 | tf_op jit(solution)/shard_map/all_gather | solution.py:44
  7.3 94.6 %all-gather.7.cloned.1.call-start = ((), (), s32[]{:S(2)}) async-start(), calls=%async_computation.3 | async-start | bytes 5242880 | tf_op jit(solution)/shard_map/all_gather | solution.py:61
  11.7 3.8 collective-permute-start
  14.1 5.2 %collective-permute-start.1 = (bf16[8,2048]{1,0:T(8,128)(2,1)S(1)}, bf16[8,2048]{1,0:T(8,128)(2,1)S(1)}, u32[]{:S(2)}, u32[]{:S(2)}) collective-permute-start(bf16[8,2048]{1,0:T(8,128)(2,1)S(1)} %get-tuple-element.12), channel_id=1, source_target_pairs={{1,0},{2,1},{3,2},{5,4},{6,5},{7,6},{9,8},{10,9},{11,10},{13,12},{... | collective-permute-start | bytes 98312 | tf_op jit(solution)/shard_map/ppermute | solution.py:20
  20.1 1.2 copy-start.1
  61.3 1.9 copy-start.3
  63.0 2.0 copy-start.9
  64.9 1.1 copy-start.4
  64.9 1.2 copy-start.5
  65.4 1.3 copy-start
  65.4 1.3 copy-start.6
  66.7 0.7 copy-start.7
  68.7 160.2 %all-gather.9.cloned.1.call-start = ((), (), s32[]{:S(2)}) async-start(), calls=%async_computation.4 | async-start | bytes 9437184 | tf_op jit(solution)/shard_map/all_gather | solution.py:65
  69.4 284.5 %all-gather.11.cloned.1.call-start = ((), (), s32[]{:S(2)}) async-start(), calls=%async_computation.5 | async-start | bytes 9437184 | tf_op jit(solution)/shard_map/all_gather | solution.py:71
  70.0 352.1 %reduce-scatter.2.cloned.1.call-start = ((), (), s32[]{:S(2)}) async-start(), calls=%async_computation.6 | async-start | bytes 5242880 | tf_op jit(solution)/shard_map/reduce_scatter | solution.py:73
  379.5 50.1 %copy-start.8 = (f32[512]{0:T(512)S(1)}, f32[512]{0:T(512)}, u32[]{:S(2)}) copy-start(f32[512]{0:T(512)} %param.15) | copy-start | bytes 6148
  422.1 7.5 %copy-start.2 = (bf16[1024,512]{1,0:T(8,128)(2,1)S(1)}, bf16[1024,512]{1,0:T(8,128)(2,1)}, u32[]{:S(2)}) copy-start(bf16[1024,512]{1,0:T(8,128)(2,1)} %reduce-scatter.2.cloned.1.call-done) | copy-start | bytes 3145732
Sparse Core Ops, SparseCore 0:
  9.5 51.7 all-gather.4
  68.8 32.9 all-gather.6
  103.9 124.9 all-gather.8
  230.7 123.1 all-gather.10
  379.5 42.5 reduce-scatter.1
where the time goes:
time: 438 us
  waiting for transfers between devices  354 us (81%)
  matrix products  29.5 us (7%)
  blocking collectives  22.8 us (5%)
  between operations  13.3 us (3%)
  other arithmetic  10.2 us (2%)
    all_gather x1, waiting for transfers between devices, local(): lax.all_gather(w_up, 'fs', axis=1, tiled=True)  127 us
    all_gather x1, waiting for transfers between devices, local(): lax.all_gather(w_down, 'fs', axis=1, tiled=True)  125 us
    all_gather x1, waiting for transfers between devices, local(): full_pool = lax.all_gather(pool_weight, 'fs', axis=1, tiled=True)  38.8 us
    all_gather x1, waiting for transfers between devices, local(): all_inner = lax.all_gather(inner, 'tp', axis=0, tiled=True)  31.8 us
    reduce_scatter x1, waiting for transfers between devices, local(): lax.psum_scatter(partial_terms.astype(jnp.bfloat16), 'tp', scatter_dimens...  25.6 us
    dot_general x1, matrix products, local(): jnp.dot(hidden, lax.all_gather(w_down, 'fs', axis=1, tiled=True), preferr...  25.5 us
    all_to_all x1, blocking collectives, local(): lax.all_to_all(first_sum, 'tp', split_axis=1, concat_axis=0, tiled=True)  17 us
  transfers between devices with their start and end apart: 7, of which 6 were waited for; matrix products, arithmetic and copies ran while one was open for 1% of the time, Pallas kernels for 0%

commit v1 on v0

--- a/solution.py
+++ b/solution.py
@@ -58,7 +58,12 @@
     mixed = jnp.concatenate(pieces, axis=1) * pool_scale
     first_sum = (inputs + mixed).astype(jnp.bfloat16)
     inner = rms_scale(first_sum.astype(jnp.float32), gain_mlp).astype(jnp.bfloat16)
-    all_inner = lax.all_gather(inner, "tp", axis=0, tiled=True)
+    ring = [inner]
+    for hop in range(3):
+        ring.append(lax.ppermute(ring[-1], "tp", [(dev, (dev + 1) % 4) for dev in range(4)]))
+    all_inner = jnp.roll(
+        jnp.concatenate(ring[::-1], axis=0), (lax.axis_index("tp") + 1) * ring[0].shape[0], axis=0
+    )
     contract = (((1,), (1,)), ((), ()))
     pre = lax.dot_general(
         all_inner,

time: 438 us -> 396 us (0.904)
  waiting for transfers between devices: 354 us -> 303 us
  local copies, waits for them, and re-layouts: 3.79 us -> 13.6 us
    all_gather x1, waiting for transfers between devices: 127 us -> 64.7 us  [local(): lax.all_gather(w_up, 'fs', axis=1, tiled=True)]
    ppermute x0 -> x3, waiting for transfers between devices: none -> 42.8 us  [local(): lax.ppermute(ring[-1], 'tp', [(dev, (dev + 1) % 4) for dev in range(4)])]
    all_gather x1 -> x0, waiting for transfers between devices: 31.8 us -> none  [local(): all_inner = lax.all_gather(inner, 'tp', axis=0, tiled=True)]
    unnamed x20 -> x30, local copies, waits for them, and re-layouts: 2.56 us -> 12.4 us
  transfers between devices with their start and end apart: 7 -> 9, of which waited for: 6 -> 8; matrix products, arithmetic and copies ran while one was open for 1% -> 5% of each run, Pallas kernels for 0% -> 0%
where the time goes in v1:
time: 396 us
  waiting for transfers between devices  303 us (77%)
  matrix products  29.7 us (8%)
  blocking collectives  22.8 us (6%)
  local copies, waits for them, and re-layouts  13.6 us (3%)
  between operations  13.4 us (3%)
  other arithmetic  9.4 us (2%)
    all_gather x1, waiting for transfers between devices, local(): lax.all_gather(w_down, 'fs', axis=1, tiled=True)  125 us
    all_gather x1, waiting for transfers between devices, local(): lax.all_gather(w_up, 'fs', axis=1, tiled=True)  64.7 us
    ppermute x3, waiting for transfers between devices, local(): lax.ppermute(ring[-1], 'tp', [(dev, (dev + 1) % 4) for dev in range(4)])  42.8 us
    all_gather x1, waiting for transfers between devices, local(): full_pool = lax.all_gather(pool_weight, 'fs', axis=1, tiled=True)  38.7 us
    reduce_scatter x1, waiting for transfers between devices, local(): lax.psum_scatter(partial_terms.astype(jnp.bfloat16), 'tp', scatter_dimens...  25.6 us
    dot_general x1, matrix products, local(): jnp.dot(hidden, lax.all_gather(w_down, 'fs', axis=1, tiled=True), preferr...  25.5 us
    all_to_all x1, blocking collectives, local(): lax.all_to_all(first_sum, 'tp', split_axis=1, concat_axis=0, tiled=True)  17 us
    unnamed x30, local copies, waits for them, and re-layouts  12.4 us
  transfers between devices with their start and end apart: 9, of which 8 were waited for; matrix products, arithmetic and copies ran while one was open for 5% of the time, Pallas kernels for 0%

profile of v1, /device:TPU:0, one launch (start us, length us, event | category | flops | bytes accessed | tf_op | source)
XLA Modules:
  0.0 395.7 jit_solution(4421293765592188307)
XLA Ops:
  6.5 0.7 all-gather.4.cloned.1.call-update
  7.3 0.7 all-gather.6.cloned.1.call-update
  8.1 0.7 all-gather.8.cloned.1.call-update
  9.1 1.6 fusion.39
  10.7 2.4 collective-permute-start
  13.1 1.3 collective-permute-start.1
  14.5 3.8 collective-permute-done.1
  19.1 1.2 copy-done.1
  20.5 1.0 copy-done.2
  21.5 1.1 fusion.41
  22.6 38.7 %all-gather.4.cloned.1.call-done = bf16[4,512,512]{2,1,0:T(8,128)(2,1)} async-done(((bf16[4,64,512]{2,1,0:T(8,128)(2,1)}), bf16[4,512,512]{2,1,0:T(8,128)(2,1)}) %all-gather.4.cloned.1.call-update) | async-done | bytes 2097168 | tf_op jit(solution)/shard_map/all_gather | solution.py:44
  61.3 1.9 fusion.19
  63.4 1.7 fusion.17
  67.8 14.2 %collective-permute-done.2 = bf16[256,2048]{1,0:T(8,128)(2,1)S(1)} collective-permute-done((bf16[256,2048]{1,0:T(8,128)(2,1)S(1)}, bf16[256,2048]{1,0:T(8,128)(2,1)S(1)}, u32[]{:S(2)}, u32[]{:S(2)}) %collective-permute-start.2) | collective-permute-done | bytes 1048608 | tf_op jit(solution)/shard_map/ppermute | solution.py:63
  82.0 14.2 %collective-permute-done.3 = bf16[256,2048]{1,0:T(8,128)(2,1)S(1)} collective-permute-done((bf16[256,2048]{1,0:T(8,128)(2,1)S(1)}, bf16[256,2048]{1,0:T(8,128)(2,1)S(1)}, u32[]{:S(2)}, u32[]{:S(2)}) %collective-permute-start.3) | collective-permute-done | bytes 1048608 | tf_op jit(solution)/shard_map/ppermute | solution.py:63
  96.2 14.3 %collective-permute-done.4 = bf16[256,2048]{1,0:T(8,128)(2,1)} collective-permute-done((bf16[256,2048]{1,0:T(8,128)(2,1)S(1)}, bf16[256,2048]{1,0:T(8,128)(2,1)}, u32[]{:S(2)}, u32[]{:S(2)}) %collective-permute-start.4) | collective-permute-done | bytes 1048608 | tf_op jit(solution)/shard_map/ppermute | solution.py:63
  110.5 2.3 constant_dynamic-update-slice_fusion.7
  112.9 1.0 constant_dynamic-update-slice_fusion.6
  113.9 1.1 constant_dynamic-update-slice_fusion.5
  115.0 1.3 constant_dynamic-update-slice_fusion.4
  116.3 2.4 constant_dynamic-update-slice_fusion.3
  118.7 1.1 constant_dynamic-update-slice_fusion.2
  119.7 1.1 constant_dynamic-update-slice_fusion.1
  120.8 1.3 constant_dynamic-update-slice_fusion
  122.2 64.7 %all-gather.6.cloned.1.call-done = bf16[2048,2048]{1,0:T(8,128)(2,1)} async-done(((bf16[2048,256]{1,0:T(8,128)(2,1)}), bf16[2048,2048]{1,0:T(8,128)(2,1)}) %all-gather.6.cloned.1.call-update) | async-done | bytes 8388624 | tf_op jit(solution)/shard_map/all_gather | solution.py:70
  186.9 125.2 %all-gather.8.cloned.1.call-done = bf16[2048,2048]{1,0:T(8,128)(2,1)} async-done(((bf16[2048,256]{1,0:T(8,128)(2,1)}), bf16[2048,2048]{1,0:T(8,128)(2,1)}) %all-gather.8.cloned.1.call-update) | async-done | bytes 8388624 | tf_op jit(solution)/shard_map/all_gather | solution.py:76
  312.1 25.5 %fusion.4 = bf16[1024,2048]{1,0:T(8,128)(2,1)} fusion(bf16[2048,2048]{1,0:T(8,128)(2,1)} %all-gather.8.cloned.1.call-done, bf16[2048,2048]{1,0:T(8,128)(2,1)} %all-gather.6.cloned.1.call-done, bf16[2048,2048]{1,0:T(8,128)(2,1)} %constant_dynamic-update-slice_fusion, s32[]{:T(128)S(6)} %select_n.64), kind=kOutput, calls=%fused_computation.3 | convolution fusion | flops 17188257792 | bytes 25165828 | tf_op jit(solution)/shard_map/dot_general | solution.py:75
  337.7 17.0 %all_to_all.13 = bf16[256,4,512]{2,0,1:T(8,128)(2,1)S(1)} all-to-all(bf16[256,4,512]{2,0,1:T(8,128)(2,1)S(1)} %bitcast.27), channel_id=1, replica_groups=mesh['fs'=8,'tp'=4] {'tp'}, dimensions={1} | all-to-all | bytes 2097152 | tf_op jit(solution)/shard_map/all_to_all | solution.py:81
  354.7 25.6 %reduce-scatter.2.cloned.1.call-done = bf16[1024,512]{1,0:T(8,128)(2,1)} async-done(((bf16[1024,2048]{1,0:T(8,128)(2,1)}), bf16[1024,512]{1,0:T(8,128)(2,1)}) %reduce-scatter.2.cloned.1.call-update) | async-done | bytes 1048592 | tf_op jit(solution)/shard_map/reduce_scatter | solution.py:78
  380.3 1.7 multiply_reduce_fusion
  382.0 5.8 %psum.7 = f32[1024]{0:T(1024)S(1)} all-reduce(f32[1024]{0:T(1024)S(1)} %multiply_reduce_fusion), channel_id=1, replica_groups=mesh['fs'=8,'tp'=4] {'tp'}, use_global_device_ids=true, to_apply=%region_4.5 | all-reduce | flops 1024 | bytes 8192 | tf_op jit(solution)/shard_map/psum | solution.py:83
  387.8 1.4 multiply_convert_fusion.1
  (48 shorter events, 4.3 us)
Async XLA Ops:
  6.5 2.3 copy-start
  6.5 2.6 copy-start.8
  6.5 54.8 %all-gather.4.cloned.1.call-start = ((), (), s32[]{:S(2)}) async-start(), calls=%async_computation.2 | async-start | bytes 2359296 | tf_op jit(solution)/shard_map/all_gather | solution.py:44
  7.3 179.6 %all-gather.6.cloned.1.call-start = ((), (), s32[]{:S(2)}) async-start(), calls=%async_computation.3 | async-start | bytes 9437184 | tf_op jit(solution)/shard_map/all_gather | solution.py:70
  8.0 304.1 %all-gather.8.cloned.1.call-start = ((), (), s32[]{:S(2)}) async-start(), calls=%async_computation.4 | async-start | bytes 9437184 | tf_op jit(solution)/shard_map/all_gather | solution.py:76
  8.7 371.6 %reduce-scatter.2.cloned.1.call-start = ((), (), s32[]{:S(2)}) async-start(), calls=%async_computation.5 | async-start | bytes 5242880 | tf_op jit(solution)/shard_map/reduce_scatter | solution.py:78
  10.7 3.8 collective-permute-start
  13.1 5.2 %collective-permute-start.1 = (bf16[8,2048]{1,0:T(8,128)(2,1)S(1)}, bf16[8,2048]{1,0:T(8,128)(2,1)S(1)}, u32[]{:S(2)}, u32[]{:S(2)}) collective-permute-start(bf16[8,2048]{1,0:T(8,128)(2,1)S(1)} %get-tuple-element.12), channel_id=1, source_target_pairs={{1,0},{2,1},{3,2},{5,4},{6,5},{7,6},{9,8},{10,9},{11,10},{13,12},{... | collective-permute-start | bytes 98312 | tf_op jit(solution)/shard_map/ppermute | solution.py:20
  19.1 1.2 copy-start.1
  20.5 1.0 copy-start.2
  61.3 2.1 copy-start.4
  63.2 2.0 copy-start.11
  65.1 1.1 copy-start.5
  65.1 1.2 copy-start.6
  65.5 1.1 copy-start.9
  66.7 0.7 copy-start.7
  67.7 14.3 %collective-permute-start.2 = (bf16[256,2048]{1,0:T(8,128)(2,1)S(1)}, bf16[256,2048]{1,0:T(8,128)(2,1)S(1)}, u32[]{:S(2)}, u32[]{:S(2)}) collective-permute-start(bf16[256,2048]{1,0:T(8,128)(2,1)S(1)} %fusion.9), channel_id=1, source_target_pairs={{0,1},{1,2},{2,3},{3,0},{4,5},{5,6},{6,7},{7,4},{8,9},{9,10},{10,1... | collective-permute-start | bytes 3145736 | tf_op jit(solution)/shard_map/ppermute | solution.py:63
  82.0 14.2 %collective-permute-start.3 = (bf16[256,2048]{1,0:T(8,128)(2,1)S(1)}, bf16[256,2048]{1,0:T(8,128)(2,1)S(1)}, u32[]{:S(2)}, u32[]{:S(2)}) collective-permute-start(bf16[256,2048]{1,0:T(8,128)(2,1)S(1)} %collective-permute-done.2), channel_id=1, source_target_pairs={{0,1},{1,2},{2,3},{3,0},{4,5},{5,6},{6,7},{7,4},{8,9},{9,10},{10,1... | collective-permute-start | bytes 3145736 | tf_op jit(solution)/shard_map/ppermute | solution.py:63
  96.2 14.3 %collective-permute-start.4 = (bf16[256,2048]{1,0:T(8,128)(2,1)S(1)}, bf16[256,2048]{1,0:T(8,128)(2,1)}, u32[]{:S(2)}, u32[]{:S(2)}) collective-permute-start(bf16[256,2048]{1,0:T(8,128)(2,1)S(1)} %collective-permute-done.3), channel_id=1, source_target_pairs={{0,1},{1,2},{2,3},{3,0},{4,5},{5,6},{6,7},{7,4},{8,9},{9,10},{10,1... | collective-permute-start | bytes 3145736 | tf_op jit(solution)/shard_map/ppermute | solution.py:63
  337.7 50.1 %copy-start.10 = (f32[512]{0:T(512)S(1)}, f32[512]{0:T(512)}, u32[]{:S(2)}) copy-start(f32[512]{0:T(512)} %param.15) | copy-start | bytes 6148
  380.3 7.5 %copy-start.3 = (bf16[1024,512]{1,0:T(8,128)(2,1)S(1)}, bf16[1024,512]{1,0:T(8,128)(2,1)}, u32[]{:S(2)}) copy-start(bf16[1024,512]{1,0:T(8,128)(2,1)} %reduce-scatter.2.cloned.1.call-done) | copy-start | bytes 3145732
Sparse Core Ops, SparseCore 0:
  9.5 51.7 all-gather.3
  63.4 123.4 all-gather.5
  188.9 123.1 all-gather.7
  337.7 42.5 reduce-scatter.1
